TPU v7x, 256 devices: a 4x2x16 block of a 4x16x16 slice. The times are simulated.
256 devices in a mesh: grp: 2 (over y), ep: 64 (over z, x), tp: 2 (over core).
Axes of the slice: x: 4, y: 2, z: 16, core: 2. Of those that a mesh axis runs over, the one named last changes fastest.
The devices are a block of a 4x16x16 slice.
Arguments:
- tokens: bfloat16 [32768, 2048], P(('grp', 'ep'), 'tp'), parts along dimension 0, may hold values from -6 to 6
- norm_gain: bfloat16 [2048], P('tp'), may hold values from 0.099609375 to 1.8984375
- w_gate: bfloat16 [64, 2048, 1024], P('ep', None, 'tp'), may hold values from -0.125 to 0.125
- w_up: bfloat16 [64, 2048, 1024], P('ep', None, 'tp'), may hold values from -0.125 to 0.125
- w_down: bfloat16 [64, 1024, 2048], P('ep', 'tp'), may hold values from -0.1875 to 0.1875
- expert_ids: int32 [32768, 2], P(('grp', 'ep')), parts along dimension 0, may hold values from 0 to 63, as said below
- combine: float32 [32768, 2], P(('grp', 'ep')), parts along dimension 0, may hold values from 0.1 to 1
- final_gain: bfloat16 [2048], P('tp'), may hold values from 0.099609375 to 1.8984375
Outputs:
- result: bfloat16 [32768, 2048], P(('grp', 'ep'), 'tp'), parts along dimension 0
There are 2 independent parts, one for each index of `grp`. A program takes and returns all parts, laid end to end along the dimension named above; an argument that names none is the same for every part. Nothing has to cross between parts.
Inputs may be any that keep to these rules, and one draw needn't show every extreme that they name: `expert_ids`: the experts form 4 groups of consecutive ids of equal size; the 2 experts of a row are different and lie in one group. Among the rows of one index of ep no expert is named more than 20 times, and in each such block some expert is named exactly 20 times.
All inputs are finite; a program needn't handle non-finite values.
Results may differ from a plain program's by a relative error of at most 0.0077.
Values may be sent and summed in bfloat16 or wider, within the bound.
No kernel may reach another device: no remote copies, remote signals or barrier semaphores. Data moves between devices by JAX's collectives and lax.ppermute only.
A program may use at most 64 MiB of HBM per device.

v0:
```python
import jax
import jax.numpy as jnp
from jax import lax
from jax.sharding import PartitionSpec as P

GROUPS = 4


def total_of_pieces(x, axis):
    parts = lax.all_gather(x, axis)
    return parts.sum(axis=0)


def split_up(x, dim, count):
    lengths = x.shape
    parts = x.reshape(*lengths[:dim], count, lengths[dim] // count, *lengths[dim + 1 :])
    return jnp.moveaxis(parts, dim, 0)


def sent_and_summed(x, axis, dim):
    parts = split_up(x, dim, lax.axis_size(axis))
    arrived = lax.all_to_all(parts, axis, split_axis=0, concat_axis=0, tiled=True)
    return arrived.astype(jnp.float32).sum(axis=0)


def body(tokens, norm_gain, w_gate, w_up, w_down, expert_ids, combine, final_gain):
    eps = 1e-06
    tok_dev, half = tokens.shape
    n_ep = lax.axis_size("ep")
    n_tp = lax.axis_size("tp")
    width = half * n_tp
    exp_dev = w_gate.shape[0]
    experts = exp_dev * n_ep
    per_group = experts // GROUPS
    capacity = tok_dev // 8 * 5 * 2 // per_group
    top = expert_ids.shape[1]
    narrow = tokens.astype(jnp.float32)
    squares = total_of_pieces(jnp.sum(narrow * narrow, axis=1), "tp")
    scale = lax.rsqrt(squares[:, None] / width + eps)
    normed = (narrow * scale * norm_gain.astype(jnp.float32)).astype(jnp.bfloat16)
    columns = normed.shape[1]
    flat = expert_ids.reshape(-1)
    onehot = (flat[:, None] == jnp.arange(experts, dtype=jnp.int32)[None, :]).astype(jnp.int32)
    ranking = jnp.sum(jnp.cumsum(onehot, axis=0) * onehot, axis=1) - 1
    target = flat * capacity + ranking
    sources = jnp.arange(tok_dev * top, dtype=jnp.int32) // top
    owner = jnp.full((experts * capacity,), tok_dev, jnp.int32).at[target].set(sources)
    padded = jnp.concatenate([normed, jnp.zeros((1, columns), jnp.bfloat16)], axis=0)
    outgoing = padded[owner].reshape(n_ep, exp_dev * capacity, columns)
    arrived = lax.all_to_all(outgoing, "ep", split_axis=0, concat_axis=0, tiled=True)
    rows = (
        arrived.reshape(n_ep, exp_dev, capacity, columns)
        .transpose(1, 0, 2, 3)
        .reshape(exp_dev, n_ep * capacity, columns)
    )
    piece = lax.all_gather(rows, "tp", axis=2, tiled=True)
    gate = jnp.einsum("erd,edf->erf", piece, w_gate, preferred_element_type=jnp.float32)
    upper = jnp.einsum("erd,edf->erf", piece, w_up, preferred_element_type=jnp.float32)
    hidden = (jax.nn.silu(gate) * upper).astype(jnp.bfloat16)
    partial_out = jnp.einsum(
        "erf,efd->erd", hidden, w_down, preferred_element_type=jnp.float32
    ).astype(jnp.bfloat16)
    shares = sent_and_summed(partial_out, "tp", 2).astype(jnp.bfloat16)
    homeward = (
        shares.reshape(exp_dev, n_ep, capacity, half)
        .transpose(1, 0, 2, 3)
        .reshape(n_ep, exp_dev * capacity, half)
    )
    returned = lax.all_to_all(homeward, "ep", split_axis=0, concat_axis=0, tiled=True).reshape(
        experts * capacity, half
    )
    picked = returned[target].astype(jnp.float32).reshape(tok_dev, top, half)
    mixed = jnp.sum(picked * combine[:, :, None], axis=1)
    totals = total_of_pieces(jnp.sum(mixed * mixed, axis=1), "tp")
    norm = lax.rsqrt(totals[:, None] / width + eps)
    return (mixed * norm * final_gain.astype(jnp.float32)).astype(jnp.bfloat16)


def solution(mesh):
    placed = (
        P(("grp", "ep"), "tp"),
        P("tp"),
        P("ep", None, "tp"),
        P("ep", None, "tp"),
        P("ep", "tp", None),
        P(("grp", "ep"), None),
        P(("grp", "ep"), None),
        P("tp"),
    )
    return jax.shard_map(
        body, mesh=mesh, in_specs=placed, out_specs=P(("grp", "ep"), "tp"), check_vma=False
    )
```

profile of v0, /device:TPU:33, one launch (start us, length us, event | category | flops | bytes accessed | tf_op | source)
XLA Modules:
  0.0 464.1 jit_solution(18118570353789319803)
XLA Ops:
  6.5 0.0 copy-start
  6.6 0.0 all-gather.6.cloned.1.call-start
  6.6 1.0 copy.16
  7.5 0.1 eq.29
  7.7 0.1 eq.25
  7.8 0.7 broadcast_multiply_fusion
  8.5 1.2 reduce-window.6
  9.7 0.2 slice_reduce_fusion
  10.0 0.1 fusion.21
  10.1 0.1 copy.15
  10.3 0.1 mul.81
  10.4 2.5 scatter_custom_fusion
  12.9 1.2 fusion.17
  14.1 21.9 %all-gather.2 = f32[2,1,256]{2,1,0:T(1,128)S(1)} all-gather(f32[1,1,256]{2,1,0:T(1,128)S(1)} %bitcast.48), channel_id=2, replica_groups=mesh['grp'=2,'ep'=64,'tp'=2] {'tp'}, dimensions={0}, use_global_device_ids=true | all-gather | bytes 3072 | tf_op jit(solution)/shard_map/all_gather | solution.py:10
  36.1 0.7 convert_element_type.38
  36.8 1.2 fusion.19
  38.1 5.1 %gather_fusion = bf16[1280,1024]{1,0:T(8,128)(2,1)} fusion(bf16[257,1024]{1,0:T(8,128)(2,1)S(1)} %concatenate.3, s32[2048]{0:T(1024)S(1)} %pad_clamp_fusion), kind=kCustom, calls=%fused_computation | custom fusion | bytes 5248000 | tf_op jit(solution)/shard_map/gather | solution.py:49
  43.1 5.2 %reshape.113 = bf16[64,20,1024]{2,1,0:T(8,128)(2,1)} reshape(bf16[1280,1024]{1,0:T(8,128)(2,1)} %gather_fusion) | data formatting | bytes 5242880 | tf_op jit(solution)/shard_map/reshape | solution.py:49
  48.3 149.8 %all_to_all.15 = bf16[64,20,1024]{2,1,0:T(8,128)(2,1)} all-to-all(bf16[64,20,1024]{2,1,0:T(8,128)(2,1)} %reshape.113), channel_id=1, replica_groups=mesh['grp'=2,'ep'=64,'tp'=2] {'ep'}, dimensions={0} | all-to-all | bytes 5242880 | tf_op jit(solution)/shard_map/all_to_all | solution.py:50
  198.1 5.2 %reshape_transpose_reshape.6 = bf16[1,1280,1024]{2,1,0:T(8,128)(2,1)} reshape(bf16[64,20,1024]{2,1,0:T(8,128)(2,1)} %all_to_all.15) | data formatting | bytes 5242880 | tf_op jit(solution)/shard_map/reshape;transpose;reshape | solution.py:54
  203.3 0.1 all-gather.6.cloned.1.call-update
  203.3 21.7 %all-gather.6.cloned.1.call-done = bf16[1,1280,2048]{2,1,0:T(8,128)(2,1)} async-done(((bf16[1,1280,1024]{2,1,0:T(8,128)(2,1)}), bf16[1,1280,2048]{2,1,0:T(8,128)(2,1)}) %all-gather.6.cloned.1.call-update) | async-done | bytes 5242896 | tf_op jit(solution)/shard_map/all_gather | solution.py:56
  225.0 7.6 %fusion.2 = f32[1280,512]{1,0:T(8,128)} fusion(bf16[1,1280,2048]{2,1,0:T(8,128)(2,1)} %all-gather.6.cloned.1.call-done, bf16[1,2048,512]{2,1,0:T(8,128)(2,1)} %param.10), kind=kOutput, calls=%fused_computation.6 | convolution fusion | flops 2684354560 | bytes 9961472 | tf_op jit(solution)/shard_map/erd,edf->erf/dot_general | solution.py:57
  232.6 0.0 copy-done
  232.6 10.3 %convolution_convert_fusion = bf16[1280,2048]{1,0:T(8,128)(2,1)} fusion(bf16[1,512,2048]{2,1,0:T(8,128)(2,1)S(1)} %copy-done, bf16[1,1280,2048]{2,1,0:T(8,128)(2,1)} %all-gather.6.cloned.1.call-done, f32[1280,512]{1,0:T(8,128)} %fusion.2, bf16[1,2048,512]{2,1,0:T(8,128)(2,1)} %param.11), kind=kOutput, calls=%fused_computation.3 | convolution fusion | flops 5375262720 | bytes 17301504 | tf_op jit(solution)/shard_map/erf,efd->erd/dot_general | solution.py:60
  242.9 9.5 %reshape.118 = bf16[1,1280,2,1024]{3,2,1,0:T(2,128)(2,1)} reshape(bf16[1280,2048]{1,0:T(8,128)(2,1)} %convolution_convert_fusion) | data formatting | bytes 10485760 | tf_op jit(solution)/shard_map/reshape | solution.py:16
  252.4 4.1 copy.24
  256.5 9.0 %all_to_all.16 = bf16[2,1,1280,1024]{3,2,1,0:T(8,128)(2,1)} all-to-all(bf16[2,1,1280,1024]{3,2,1,0:T(8,128)(2,1)S(1)} %bitcast.44), channel_id=1, replica_groups=mesh['grp'=2,'ep'=64,'tp'=2] {'tp'}, dimensions={0} | all-to-all | bytes 10485760 | tf_op jit(solution)/shard_map/all_to_all | solution.py:22
  265.5 6.2 %reduce_sum.69 = bf16[1280,1024]{1,0:T(8,128)(2,1)} reduce(bf16[2,1,1280,1024]{3,2,1,0:T(8,128)(2,1)} %all_to_all.16, bf16[]{:T(256)} %constant.38.clone.1), dimensions={0,1}, to_apply=%region_6.7 | reduce | flops 1310720 | bytes 7864322 | tf_op jit(solution)/shard_map/reduce_sum | solution.py:23
  271.7 5.1 %reshape_transpose_reshape.7 = bf16[64,20,1024]{2,1,0:T(8,128)(2,1)} reshape(bf16[1280,1024]{1,0:T(8,128)(2,1)} %reduce_sum.69) | data formatting | bytes 5242880 | tf_op jit(solution)/shard_map/reshape;transpose;reshape | solution.py:67
  276.9 0.0 copy-start.1
  276.9 0.0 copy-start.2
  276.9 16.3 %all-to-all-start.2 = ((bf16[64,20,1024]{2,1,0:T(8,128)(2,1)}), bf16[64,20,1024]{2,1,0:T(8,128)(2,1)}, u32[]{:S(2)}, u32[]{:S(2)}) async-start(bf16[64,20,1024]{2,1,0:T(8,128)(2,1)} %reshape_transpose_reshape.7), calls=%async_computation.2 | async-start | bytes 6291456 | tf_op jit(solution)/shard_map/all_to_all | solution.py:69
  293.2 0.0 copy-done.1
  293.2 0.1 copy.20
  293.3 0.0 copy-done.2
  293.4 138.9 %all-to-all-done.2 = bf16[64,20,1024]{2,1,0:T(8,128)(2,1)} async-done(((bf16[64,20,1024]{2,1,0:T(8,128)(2,1)}), bf16[64,20,1024]{2,1,0:T(8,128)(2,1)}, u32[]{:S(2)}, u32[]{:S(2)}) %all-to-all-start.2) | async-done | bytes 2621472 | tf_op jit(solution)/shard_map/all_to_all | solution.py:69
  432.3 5.2 %reshape.119 = bf16[1280,1024]{1,0:T(8,128)(2,1)} reshape(bf16[64,20,1024]{2,1,0:T(8,128)(2,1)} %all-to-all-done.2) | data formatting | bytes 5242880 | tf_op jit(solution)/shard_map/reshape | solution.py:69
  437.4 4.8 %gather_fusion.1 = bf16[512,1024]{1,0:T(8,128)(2,1)S(1)} fusion(bf16[1280,1024]{1,0:T(8,128)(2,1)} %reshape.119, s32[1024]{0:T(1024)S(1)} %pad_clamp_fusion.1), kind=kCustom, calls=%fused_computation.1 | custom fusion | bytes 2099200 | tf_op jit(solution)/shard_map/gather | solution.py:72
  442.2 2.4 reshape.120
  444.6 4.3 multiply_reduce_fusion
  448.9 0.1 multiply_reduce_fusion.1
  449.1 7.2 %all-gather.3 = f32[2,1,256]{2,1,0:T(1,128)S(1)} all-gather(f32[1,1,256]{2,1,0:T(1,128)S(1)} %bitcast.49), channel_id=3, replica_groups=mesh['grp'=2,'ep'=64,'tp'=2] {'tp'}, dimensions={0}, use_global_device_ids=true | all-gather | bytes 3072 | tf_op jit(solution)/shard_map/all_gather | solution.py:10
  456.2 1.0 multiply_convert_fusion
  (15 shorter events, 0.2 us)
Async XLA Ops:
  6.5 226.0 %copy-start = (bf16[1,512,2048]{2,1,0:T(8,128)(2,1)S(1)}, bf16[1,512,2048]{2,1,0:T(8,128)(2,1)}, u32[]{:S(2)}) copy-start(bf16[1,512,2048]{2,1,0:T(8,128)(2,1)} %param.12) | copy-start | bytes 6291460
  6.6 218.5 %all-gather.6.cloned.1.call-start = ((), (), s32[]{:S(2)}) async-start(), calls=%async_computation.3 | async-start | bytes 7864320 | tf_op jit(solution)/shard_map/all_gather | solution.py:56
  276.9 16.3 %copy-start.1 = (f32[256,2]{0,1:T(2,128)S(1)}, f32[256,2]{0,1:T(2,128)}, u32[]{:S(2)}) copy-start(f32[256,2]{0,1:T(2,128)} %param.14) | copy-start | bytes 6148
  276.9 16.5 %copy-start.2 = (bf16[1024]{0:T(1024)(128)(2,1)S(1)}, bf16[1024]{0:T(1024)(128)(2,1)}, u32[]{:S(2)}) copy-start(bf16[1024]{0:T(1024)(128)(2,1)} %param.15) | copy-start | bytes 6148
  276.9 155.4 %all-to-all-start.2 = ((bf16[64,20,1024]{2,1,0:T(8,128)(2,1)}), bf16[64,20,1024]{2,1,0:T(8,128)(2,1)}, u32[]{:S(2)}, u32[]{:S(2)}) async-start(bf16[64,20,1024]{2,1,0:T(8,128)(2,1)} %reshape_transpose_reshape.7), calls=%async_computation.2 | async-start | bytes 6291456 | tf_op jit(solution)/shard_map/all_to_all | solution.py:69
Sparse Core Ops, SparseCore 0:
  203.4 21.5 all-gather.5
where the time goes:
time: 465 us; the launch traced here: 464 us
  blocking collectives  188 us (40%)
  waiting for transfers between devices  161 us (35%)
  local copies, waits for them, and re-layouts  50.9 us (11%)
  matrix products  17.9 us (4%)
  other arithmetic  16.9 us (4%)
  starting transfers between devices  16.3 us (4%)
  between operations  13.6 us (3%)
    all_to_all x1, blocking collectives, body(): lax.all_to_all(outgoing, 'ep', split_axis=0, concat_axis=0, tiled=True)  150 us
    all_to_all x1, waiting for transfers between devices, body(): lax.all_to_all(homeward, 'ep', split_axis=0, concat_axis=0, tiled=True)  139 us
    all_gather x2, blocking collectives, total_of_pieces(): parts = lax.all_gather(x, axis)  29.1 us
    all_gather x1, waiting for transfers between devices, body(): piece = lax.all_gather(rows, 'tp', axis=2, tiled=True)  21.7 us
    all_to_all x1, starting transfers between devices, body(): lax.all_to_all(homeward, 'ep', split_axis=0, concat_axis=0, tiled=True)  16.3 us
    reshape x2, local copies, waits for them, and re-layouts, split_up(): x.reshape(*lengths[:dim], count, lengths[dim] // count, *lengths[dim + 1:])  13.6 us
    dot_general x1, matrix products, body(): jnp.einsum('erf,efd->erd', hidden, w_down, preferred_element_type=jnp.flo...  10.3 us
  transfers between devices with their start and end apart: 2, of which 2 were waited for; matrix products, arithmetic and copies ran while one was open for 0% of the time, Pallas kernels for 0%

commit v1 on v0

--- a/solution.py
+++ b/solution.py
@@ -1,9 +1,21 @@
+import functools
 import jax
 import jax.numpy as jnp
 from jax import lax
 from jax.sharding import PartitionSpec as P
 
 GROUPS = 4
+
+
+def tokens_handle(x_local, net_axis):
+    sheets = []
+    for _ in range(lax.axis_size(net_axis)):
+        sheets.append(x_local)
+    clean = lax.all_to_all(jnp.stack(sheets, 0), axis_name=net_axis, split_axis=0, concat_axis=0)
+    return jnp.concatenate(clean, 2)
+
+
+_use_ladders = functools.partial(tokens_handle, net_axis="tp")
 
 
 def total_of_pieces(x, axis):
@@ -53,7 +65,7 @@
         .transpose(1, 0, 2, 3)
         .reshape(exp_dev, n_ep * capacity, columns)
     )
-    piece = lax.all_gather(rows, "tp", axis=2, tiled=True)
+    piece = _use_ladders(rows)
     gate = jnp.einsum("erd,edf->erf", piece, w_gate, preferred_element_type=jnp.float32)
     upper = jnp.einsum("erd,edf->erf", piece, w_up, preferred_element_type=jnp.float32)
     hidden = (jax.nn.silu(gate) * upper).astype(jnp.bfloat16)

time: 465 us -> 440 us (0.946)
  waiting for transfers between devices: 161 us -> 139 us
  between operations: 13.6 us -> 0.18 us
  blocking collectives: 188 us -> 201 us
  starting transfers between devices: 16.3 us -> 7.6 us
    all_gather x1 -> x0, waiting for transfers between devices: 21.7 us -> none  [body(): piece = lax.all_gather(rows, 'tp', axis=2, tiled=True)]
    all_to_all x0 -> x1, blocking collectives: none -> 13.6 us  [tokens_handle(): lax.all_to_all(jnp.stack(sheets, 0), axis_name=net_axis, split_axis=0, co...]
    all_to_all x1, starting transfers between devices: 16.3 us -> 7.6 us  [body(): lax.all_to_all(homeward, 'ep', split_axis=0, concat_axis=0, tiled=True)]
    reshape x0 -> x1, local copies, waits for them, and re-layouts: none -> 7.92 us  [tokens_handle(): return jnp.concatenate(clean, 2)]
  transfers between devices with their start and end apart: 2 -> 1, of which waited for: 2 -> 1; matrix products, arithmetic and copies ran while one was open for 0% -> 0% of each run, Pallas kernels for 0% -> 0%
where the time goes in v1:
time: 440 us; the launch traced here: 438 us
  blocking collectives  201 us (46%)
  waiting for transfers between devices  139 us (32%)
  local copies, waits for them, and re-layouts  53.7 us (12%)
  other arithmetic  18.8 us (4%)
  matrix products  17.9 us (4%)
  starting transfers between devices  7.6 us (2%)
    all_to_all x1, blocking collectives, body(): lax.all_to_all(outgoing, 'ep', split_axis=0, concat_axis=0, tiled=True)  150 us
    all_to_all x1, waiting for transfers between devices, body(): lax.all_to_all(homeward, 'ep', split_axis=0, concat_axis=0, tiled=True)  139 us
    all_gather x2, blocking collectives, total_of_pieces(): parts = lax.all_gather(x, axis)  28.4 us
    reshape x2, local copies, waits for them, and re-layouts, split_up(): x.reshape(*lengths[:dim], count, lengths[dim] // count, *lengths[dim + 1:])  13.6 us
    all_to_all x1, blocking collectives, tokens_handle(): lax.all_to_all(jnp.stack(sheets, 0), axis_name=net_axis, split_axis=0, co...  13.6 us
    dot_general x1, matrix products, body(): jnp.einsum('erf,efd->erd', hidden, w_down, preferred_element_type=jnp.flo...  10.3 us
    all_to_all x1, blocking collectives, sent_and_summed(): lax.all_to_all(parts, axis, split_axis=0, concat_axis=0, tiled=True)  9.02 us
  transfers between devices with their start and end apart: 1, of which 1 were waited for; matrix products, arithmetic and copies ran while one was open for 0% of the time, Pallas kernels for 0%

profile of v1, /device:TPU:33, one launch (start us, length us, event | category | flops | bytes accessed | tf_op | source)
XLA Modules:
  0.0 438.3 jit_solution(13814672209699792496)
XLA Ops:
  0.0 0.0 copy-start
  0.0 1.0 copy.17
  1.0 0.1 eq.29
  1.1 0.1 eq.25
  1.3 0.7 broadcast_multiply_fusion
  2.0 1.2 reduce-window.6
  3.2 0.2 slice_reduce_fusion
  3.4 0.1 fusion.11
  3.6 0.1 copy.16
  3.7 0.1 mul.81
  3.9 2.5 scatter_custom_fusion
  6.4 1.2 fusion.5
  7.6 21.9 %all-gather.2 = f32[2,1,256]{2,1,0:T(1,128)S(1)} all-gather(f32[1,1,256]{2,1,0:T(1,128)S(1)} %bitcast.44), channel_id=2, replica_groups=mesh['grp'=2,'ep'=64,'tp'=2] {'tp'}, dimensions={0}, use_global_device_ids=true | all-gather | bytes 3072 | tf_op jit(solution)/shard_map/all_gather | solution.py:22
  29.5 0.7 convert_element_type.38
  30.2 1.2 fusion.7
  31.5 5.1 %gather_fusion = bf16[1280,1024]{1,0:T(8,128)(2,1)} fusion(bf16[257,1024]{1,0:T(8,128)(2,1)S(1)} %concatenate.3, s32[2048]{0:T(1024)S(1)} %pad_clamp_fusion), kind=kCustom, calls=%fused_computation | custom fusion | bytes 5248000 | tf_op jit(solution)/shard_map/gather | solution.py:61
  36.6 5.2 %reshape.119 = bf16[64,20,1024]{2,1,0:T(8,128)(2,1)} reshape(bf16[1280,1024]{1,0:T(8,128)(2,1)} %gather_fusion) | data formatting | bytes 5242880 | tf_op jit(solution)/shard_map/reshape | solution.py:61
  41.8 149.8 %all_to_all.20 = bf16[64,20,1024]{2,1,0:T(8,128)(2,1)} all-to-all(bf16[64,20,1024]{2,1,0:T(8,128)(2,1)} %reshape.119), channel_id=1, replica_groups=mesh['grp'=2,'ep'=64,'tp'=2] {'ep'}, dimensions={0} | all-to-all | bytes 5242880 | tf_op jit(solution)/shard_map/all_to_all | solution.py:62
  191.5 5.2 %stack_reshape_transpose_reshape.4 = bf16[1,1,1280,1024]{3,2,1,0:T(8,128)(2,1)} reshape(bf16[64,20,1024]{2,1,0:T(8,128)(2,1)} %all_to_all.20) | data formatting | bytes 5242880 | tf_op jit(solution)/shard_map/stack;reshape;transpose;reshape | solution.py:14
  196.7 3.0 pad_maximum_fusion
  199.7 13.6 %all_to_all.21 = bf16[2,1,1280,1024]{3,2,1,0:T(8,128)(2,1)} all-to-all(bf16[2,1,1280,1024]{3,2,1,0:T(8,128)(2,1)S(1)} %pad_maximum_fusion), channel_id=1, replica_groups=mesh['grp'=2,'ep'=64,'tp'=2] {'tp'}, dimensions={0} | all-to-all | bytes 10485760 | tf_op jit(solution)/shard_map/all_to_all | solution.py:14
  213.3 7.9 %copy.20 = bf16[1,1280,2,1024]{1,3,2,0:T(8,128)(2,1)} copy(bf16[1,1280,2,1024]{3,1,0,2:T(8,128)(2,1)} %bitcast.37) | data formatting | bytes 10485760 | tf_op jit(solution)/shard_map/reshape | solution.py:15
  221.2 7.6 %fusion.3 = f32[1280,512]{1,0:T(8,128)} fusion(bf16[1280,2048]{0,1:T(8,128)(2,1)} %bitcast.39, bf16[1,2048,512]{2,1,0:T(8,128)(2,1)} %param.10), kind=kOutput, calls=%fused_computation.10 | convolution fusion | flops 2684354560 | bytes 9961472 | tf_op jit(solution)/shard_map/erd,edf->erf/dot_general | solution.py:69
  228.8 0.0 copy-done
  228.8 10.3 %convolution_convert_fusion = bf16[1280,2048]{1,0:T(8,128)(2,1)} fusion(bf16[1,512,2048]{2,1,0:T(8,128)(2,1)S(1)} %copy-done, bf16[1280,2048]{0,1:T(8,128)(2,1)} %bitcast.40, f32[1280,512]{1,0:T(8,128)} %fusion.3, bf16[1,2048,512]{2,1,0:T(8,128)(2,1)} %param.11), kind=kOutput, calls=%fused_computation.3 | convolution fusion | flops 5375262720 | bytes 17301504 | tf_op jit(solution)/shard_map/erf,efd->erd/dot_general | solution.py:72
  239.1 9.5 %reshape.125 = bf16[1,1280,2,1024]{3,2,1,0:T(2,128)(2,1)} reshape(bf16[1280,2048]{1,0:T(8,128)(2,1)} %convolution_convert_fusion) | data formatting | bytes 10485760 | tf_op jit(solution)/shard_map/reshape | solution.py:28
  248.6 4.1 copy.26
  252.8 9.0 %all_to_all.22 = bf16[2,1,1280,1024]{3,2,1,0:T(8,128)(2,1)} all-to-all(bf16[2,1,1280,1024]{3,2,1,0:T(8,128)(2,1)S(1)} %bitcast.38), channel_id=1, replica_groups=mesh['grp'=2,'ep'=64,'tp'=2] {'tp'}, dimensions={0} | all-to-all | bytes 10485760 | tf_op jit(solution)/shard_map/all_to_all | solution.py:34
  261.8 5.1 %reduce_sum.69 = bf16[1280,1024]{1,0:T(8,128)(2,1)S(1)} reduce(bf16[2,1,1280,1024]{3,2,1,0:T(8,128)(2,1)} %all_to_all.22, bf16[]{:T(256)} %constant.38.clone.1), dimensions={0,1}, to_apply=%region_6.7 | reduce | flops 1310720 | bytes 7864322 | tf_op jit(solution)/shard_map/reduce_sum | solution.py:35
  266.9 2.4 reshape_transpose_reshape.3
  269.3 0.0 copy-start.2
  269.3 0.0 copy-start.3
  269.3 7.6 %all-to-all-start.3 = ((bf16[64,20,1024]{2,1,0:T(8,128)(2,1)}), bf16[64,20,1024]{2,1,0:T(8,128)(2,1)}, u32[]{:S(2)}, u32[]{:S(2)}) async-start(bf16[64,20,1024]{2,1,0:T(8,128)(2,1)} %reshape_transpose_reshape.3), calls=%async_computation.3 | async-start | bytes 6291456 | tf_op jit(solution)/shard_map/all_to_all | solution.py:81
  276.9 0.0 copy-done.2
  276.9 0.1 copy.22
  277.0 0.0 copy-done.3
  277.1 139.3 %all-to-all-done.3 = bf16[64,20,1024]{2,1,0:T(8,128)(2,1)} async-done(((bf16[64,20,1024]{2,1,0:T(8,128)(2,1)}), bf16[64,20,1024]{2,1,0:T(8,128)(2,1)}, u32[]{:S(2)}, u32[]{:S(2)}) %all-to-all-start.3) | async-done | bytes 2621472 | tf_op jit(solution)/shard_map/all_to_all | solution.py:81
  416.4 3.6 reshape.126
  420.0 2.8 gather_fusion.1
  422.8 0.0 copy-start.1
  422.8 3.5 reshape.127
  426.4 4.3 multiply_reduce_fusion
  430.7 0.1 multiply_reduce_fusion.1
  430.8 6.5 %all-gather.3 = f32[2,1,256]{2,1,0:T(1,128)S(1)} all-gather(f32[1,1,256]{2,1,0:T(1,128)S(1)} %bitcast.45), channel_id=3, replica_groups=mesh['grp'=2,'ep'=64,'tp'=2] {'tp'}, dimensions={0}, use_global_device_ids=true | all-gather | bytes 3072 | tf_op jit(solution)/shard_map/all_gather | solution.py:22
  437.4 1.0 multiply_convert_fusion
  438.3 0.0 copy-done.1
  (15 shorter events, 0.2 us)
Async XLA Ops:
  0.0 228.8 %copy-start = (bf16[1,512,2048]{2,1,0:T(8,128)(2,1)S(1)}, bf16[1,512,2048]{2,1,0:T(8,128)(2,1)}, u32[]{:S(2)}) copy-start(bf16[1,512,2048]{2,1,0:T(8,128)(2,1)} %param.12) | copy-start | bytes 6291460
  269.3 7.6 %copy-start.2 = (f32[256,2]{0,1:T(2,128)S(1)}, f32[256,2]{0,1:T(2,128)}, u32[]{:S(2)}) copy-start(f32[256,2]{0,1:T(2,128)} %param.14) | copy-start | bytes 6148
  269.3 7.8 %copy-start.3 = (bf16[1024]{0:T(1024)(128)(2,1)S(1)}, bf16[1024]{0:T(1024)(128)(2,1)}, u32[]{:S(2)}) copy-start(bf16[1024]{0:T(1024)(128)(2,1)} %param.15) | copy-start | bytes 6148
  269.3 147.1 %all-to-all-start.3 = ((bf16[64,20,1024]{2,1,0:T(8,128)(2,1)}), bf16[64,20,1024]{2,1,0:T(8,128)(2,1)}, u32[]{:S(2)}, u32[]{:S(2)}) async-start(bf16[64,20,1024]{2,1,0:T(8,128)(2,1)} %reshape_transpose_reshape.3), calls=%async_computation.3 | async-start | bytes 6291456 | tf_op jit(solution)/shard_map/all_to_all | solution.py:81
  422.8 15.5 %copy-start.1 = (bf16[1,512,2048]{2,1,0:T(8,128)(2,1)S(1)}, bf16[1,512,2048]{2,1,0:T(8,128)(2,1)}, u32[]{:S(2)}) copy-start(bf16[1,512,2048]{2,1,0:T(8,128)(2,1)} %param.12) | copy-start | bytes 6291460
